TPU v7x, 256 devices: a 4x2x16 block of a 4x16x16 slice. The times are simulated.
256 devices in a mesh: grp: 2 (over y), sp: 16 (over z), tp: 8 (over x, core).
Axes of the slice: x: 4, y: 2, z: 16, core: 2. Of those that a mesh axis runs over, the one named last changes fastest.
The devices are a block of a 4x16x16 slice.
Arguments:
- queries: bfloat16 [24576, 1024], P(('grp', 'sp'), 'tp'), parts along dimension 0, may hold values from -8 to 8
- keys: bfloat16 [24576, 256], P(('grp', 'sp')), parts along dimension 0, may hold values from -8 to 8
- values: bfloat16 [24576, 256], P(('grp', 'sp')), parts along dimension 0, may hold values from -6 to 6
- query_gain: float32 [128], replicated, may hold values from 0.2 to 6
- key_gain: float32 [128], replicated, may hold values from 0.2 to 6
- residual: bfloat16 [24576, 2048], P(('grp', 'sp', 'tp')), parts along dimension 0, may hold values from -6 to 6
- out_weight: bfloat16 [1024, 2048], P('tp'), may hold values from -0.1875 to 0.1875
- mix_gain: float32 [2048], replicated, may hold values from 0.1 to 1.9
- ffn_gain: float32 [2048], replicated, may hold values from 0.1 to 1.9
- gate_in: bfloat16 [2048, 5632], P('sp', 'tp'), may hold values from -0.125 to 0.125
- value_in: bfloat16 [2048, 5632], P('sp', 'tp'), may hold values from -0.125 to 0.125
- conv_gate: float32 [3, 5632], P(None, 'tp'), may hold values from -3 to 3
- conv_value: float32 [3, 5632], P(None, 'tp'), may hold values from -3 to 3
- down_t: bfloat16 [2048, 5632], P('sp', 'tp'), may hold values from -0.078125 to 0.078125
Outputs:
- layer_out: bfloat16 [24576, 2048], P(('grp', 'sp', 'tp')), parts along dimension 0
There are 2 independent parts, one for each index of `grp`. A program takes and returns all parts, laid end to end along the dimension named above; an argument that names none is the same for every part. Nothing has to cross between parts.
All inputs are finite; a program needn't handle non-finite values.
Results may differ from a plain program's by a relative error of at most 0.02.
The roundings to bfloat16 on the way count: a program that leaves them out, or rounds other values in their place, can miss the bound.
Values may be sent and summed in bfloat16 or wider, within the bound.
A program may use at most 128 MiB of HBM per device.

v0:
```python
import jax
import jax.numpy as jnp
from jax import lax
from jax.sharding import PartitionSpec as P

HEADS = 8
KVH = 2
GRID_W = 64
EPSILON = 1e-06
THETA = 10000.0


def sent_together(arrays, axis, dim, along):
    both = jnp.concatenate(arrays, axis=along)
    whole, at, gathered = (lax.all_gather(both, axis, axis=dim, tiled=True), 0, [])
    for a in arrays:
        gathered.append(lax.slice_in_dim(whole, at, at + a.shape[along], axis=along))
        at += a.shape[along]
    return tuple(gathered)


def cut_along(array, dim, size):
    before, after = (array.shape[:dim], array.shape[dim + 1 :])
    return jnp.moveaxis(array.reshape(*before, size, -1, *after), dim, 0)


def summed_on_arrival(array, axis, dim):
    tiles = cut_along(array, dim, lax.axis_size(axis))
    arrived = lax.all_to_all(tiles, axis, split_axis=0, concat_axis=0, tiled=True)
    return arrived.astype(jnp.float32).sum(axis=0)


def with_halo(block, sides, width):
    for axis, dim in sides:
        count = lax.axis_size(axis)
        forward = [(i, i + 1) for i in range(count - 1)]
        backward = [(target, source) for source, target in forward]
        low = lax.ppermute(
            lax.slice_in_dim(block, block.shape[dim] - width, None, axis=dim), axis, forward
        )
        high = lax.ppermute(lax.slice_in_dim(block, 0, width, axis=dim), axis, backward)
        block = jnp.concatenate([low, block, high], axis=dim)
    return block


def rotary_tables(positions, seq_total, head_dim):
    quarter = head_dim // 4
    inverse = THETA ** (-(2.0 * jnp.arange(quarter, dtype=jnp.float32)) / (head_dim // 2))
    grid_row = (positions // GRID_W - seq_total // GRID_W // 2).astype(jnp.float32)
    grid_col = (positions % GRID_W - GRID_W // 2).astype(jnp.float32)
    row_angle = grid_row[:, None] * inverse[None, :]
    col_angle = grid_col[:, None] * inverse[None, :]
    angle = jnp.concatenate([row_angle, row_angle, col_angle, col_angle], axis=-1)
    return (jnp.cos(angle), jnp.sin(angle))


def rotate_quarters(vector):
    first, second, third, fourth = jnp.split(vector, 4, axis=-1)
    return jnp.concatenate([-second, first, -fourth, third], axis=-1)


def prepare_heads(raw, gain, cos_table, sin_table, factor):
    floats = raw.astype(jnp.float32)
    normed = floats * lax.rsqrt(jnp.mean(floats * floats, axis=-1, keepdims=True) + EPSILON) * gain
    turned = normed * cos_table + rotate_quarters(normed) * sin_table
    return (turned * factor).astype(jnp.bfloat16)


def rms_rows(stream, gain):
    floats = stream.astype(jnp.float32)
    return floats * lax.rsqrt(jnp.mean(floats * floats, axis=-1, keepdims=True) + EPSILON) * gain


def body(
    queries,
    keys,
    values,
    query_gain,
    key_gain,
    residual,
    out_weight,
    mix_gain,
    ffn_gain,
    gate_in,
    value_in,
    conv_gate,
    conv_value,
    down_t,
):
    gate_rows, value_rows, down_rows = sent_together((gate_in, value_in, down_t), "sp", 0, 1)
    tok_rows = queries.shape[0]
    head_dim = query_gain.shape[0]
    local_heads = queries.shape[1] // head_dim
    seq_total = tok_rows * lax.axis_size("sp")
    kv_head = lax.axis_index("tp") * local_heads // (HEADS // KVH)
    positions = lax.axis_index("sp") * tok_rows + jnp.arange(tok_rows, dtype=jnp.int32)
    cos_table, sin_table = rotary_tables(positions, seq_total, head_dim)
    key_own = lax.dynamic_slice_in_dim(keys, kv_head * head_dim, head_dim, 1)
    value_own = lax.dynamic_slice_in_dim(values, kv_head * head_dim, head_dim, 1)
    key_rot = prepare_heads(key_own, key_gain, cos_table, sin_table, 1.0)
    query_rot = prepare_heads(
        queries.reshape(tok_rows, local_heads, head_dim),
        query_gain,
        cos_table[:, None, :],
        sin_table[:, None, :],
        head_dim ** (-0.5),
    )
    query_rows = jnp.transpose(query_rot, (1, 0, 2)).reshape(local_heads * tok_rows, head_dim)
    query_count = local_heads * tok_rows
    running = jnp.full((query_count, 1), -1e30, jnp.float32)
    key_piece, value_piece = sent_together((key_rot, value_own), "sp", 0, 1)
    scores = lax.dot_general(
        query_rows, key_piece, (((1,), (1,)), ((), ())), preferred_element_type=jnp.float32
    )
    newest = jnp.maximum(running, jnp.max(scores, axis=1, keepdims=True))
    weights = jnp.exp(scores - newest)
    denom = jnp.sum(weights, axis=1, keepdims=True)
    summed = jnp.dot(weights.astype(jnp.bfloat16), value_piece, preferred_element_type=jnp.float32)
    running, denom, summed = (newest, denom, summed)
    attended = (summed / denom).astype(jnp.bfloat16).reshape(local_heads, tok_rows, head_dim)
    attended = jnp.transpose(attended, (1, 0, 2)).reshape(tok_rows, local_heads * head_dim)
    block_rows = attended
    mix = summed_on_arrival(
        jnp.dot(block_rows, out_weight, preferred_element_type=jnp.float32).astype(jnp.bfloat16),
        "tp",
        0,
    )
    stream = (residual.astype(jnp.float32) + rms_rows(mix, mix_gain)).astype(jnp.bfloat16)
    normed = rms_rows(stream, ffn_gain).astype(jnp.bfloat16)
    paired = jnp.concatenate([gate_rows, value_rows], axis=1)
    upward = jnp.dot(
        lax.all_gather(normed, "tp", axis=0, tiled=True), paired, preferred_element_type=jnp.float32
    ).astype(jnp.bfloat16)
    padded = with_halo(upward, (("sp", 0),), 1).astype(jnp.float32)
    taps = jnp.concatenate([conv_gate, conv_value], axis=1)
    mixed = taps[0] * padded[:-2] + taps[1] * padded[1:-1] + taps[2] * padded[2:]
    unit_cols = conv_gate.shape[1]
    hidden = (jax.nn.gelu(mixed[:, :unit_cols], approximate=True) * mixed[:, unit_cols:]).astype(
        jnp.bfloat16
    )
    block_rows = hidden
    ffn_out = summed_on_arrival(
        lax.dot_general(
            block_rows, down_rows, (((1,), (1,)), ((), ())), preferred_element_type=jnp.float32
        ).astype(jnp.bfloat16),
        "tp",
        0,
    )
    return (stream.astype(jnp.float32) + ffn_out).astype(jnp.bfloat16)


def solution(mesh):
    return jax.shard_map(
        body,
        mesh=mesh,
        in_specs=(
            P(("grp", "sp"), "tp"),
            P(("grp", "sp"), None),
            P(("grp", "sp"), None),
            P(),
            P(),
            P(("grp", "sp", "tp"), None),
            P("tp", None),
            P(),
            P(),
            P("sp", "tp"),
            P("sp", "tp"),
            P(None, "tp"),
            P(None, "tp"),
            P("sp", "tp"),
        ),
        out_specs=P(("grp", "sp", "tp"), None),
        check_vma=False,
    )
```

profile of v0, /device:TPU:33, one launch (start us, length us, event | category | flops | bytes accessed | tf_op | source)
XLA Modules:
  0.0 345.3 jit_solution(11012669087130800998)
XLA Ops:
  6.5 0.0 copy-start
  6.6 0.0 copy-start.3
  6.6 0.0 copy-start.10
  6.6 0.0 all-gather.4.cloned.1.call-start
  6.6 1.2 fusion.55
  7.8 1.1 fusion.56
  8.9 0.0 copy-start.2
  8.9 0.0 copy-start.9
  8.9 0.4 slice_negate_fusion.1
  9.3 0.9 constant_dynamic-slice_fusion
  10.3 0.3 broadcast_multiply_fusion.1
  10.6 0.0 copy-done.3
  10.6 0.0 copy-done.10
  10.6 2.0 fusion.60
  12.6 0.8 pad_maximum_fusion.2
  13.4 0.1 all-gather.4.cloned.1.call-update
  13.4 0.1 all-gather.8.cloned.1.call-start
  13.5 1.9 pad_maximum_fusion
  15.4 0.1 all-gather.8.cloned.1.call-update
  15.5 0.1 all-gather.6.cloned.1.call-start
  15.6 0.0 copy-done.2
  15.6 0.2 fusion.48
  15.8 0.0 copy-done.9
  15.8 0.2 fusion.50
  16.0 0.4 fusion.58
  16.3 93.2 %all-gather.4.cloned.1.call-done = bf16[12288,256]{1,0:T(8,128)(2,1)} async-done(((bf16[768,256]{1,0:T(8,128)(2,1)}), bf16[12288,256]{1,0:T(8,128)(2,1)}) %all-gather.4.cloned.1.call-update) | async-done | bytes 6291472 | tf_op jit(solution)/shard_map/all_gather | solution.py:15
  109.5 16.3 %fusion.87 = (f32[768]{0:T(1024)S(1)}, f32[768,12288]{1,0:T(8,128)}) fusion(bf16[12288,256]{1,0:T(8,128)(2,1)} %all-gather.4.cloned.1.call-done, bf16[768,128]{1,0:T(8,128)(2,1)S(1)} %copy-done.2, f32[768,32]{1,0:T(8,128)S(1)} %get-tuple-element.13, f32[768,32]{1,0:T(8,128)S(1)} %get-tuple-element.14, f32[768,32]{1,0:T(8,128)S(1)} %get-tuple-element.15, ...), kind=kOutput, calls=%fused_computation.117 | convolution fusion | flops 2426731776 | bytes 41687552 | tf_op jit(solution)/shard_map/dot_general | solution.py:112
  125.9 15.4 %fusion = f32[768]{0:T(1024)S(1)} fusion(f32[768,12288]{1,0:T(8,128)} %get-tuple-element.23, f32[768]{0:T(1024)S(1)} %broadcast_maximum_fusion), kind=kLoop, calls=%fused_computation.1 | loop fusion | flops 18873600 | bytes 37754880 | tf_op jit(solution)/shard_map/reduce_sum | solution.py:117
  141.2 0.0 copy-done
  141.2 18.7 %convolution_convert_fusion.1 = bf16[768,2048]{1,0:T(8,128)(2,1)} fusion(bf16[128,2048]{1,0:T(8,128)(2,1)S(1)} %copy-done, bf16[12288,256]{1,0:T(8,128)(2,1)} %all-gather.4.cloned.1.call-done, f32[768,12288]{1,0:T(8,128)} %get-tuple-element.23, f32[768]{0:T(1024)S(1)} %broadcast_maximum_fusion, f32[768]{0:T(1024)S(1)} %fusion), kind=kOutput, calls=%fused_computation.16 | convolution fusion | flops 2839216128 | bytes 44570624 | tf_op jit(solution)/shard_map/dot_general | solution.py:124
  159.9 0.0 copy-start.4
  159.9 0.0 copy-start.7
  159.9 45.7 %all_to_all.10 = bf16[8,96,2048]{2,1,0:T(8,128)(2,1)S(1)} all-to-all(bf16[8,96,2048]{2,1,0:T(8,128)(2,1)} %bitcast.14), channel_id=1, replica_groups=mesh['grp'=2,'sp'=16,'tp'=8] {'tp'}, dimensions={0} | all-to-all | bytes 6291456 | tf_op jit(solution)/shard_map/all_to_all | solution.py:29
  205.6 0.0 copy-start.8
  205.6 0.6 convert_reduce_fusion.1
  206.2 0.1 multiply_reduce_fusion
  206.3 0.0 copy-done.4
  206.3 0.0 copy-done.7
  206.3 0.3 fusion.44
  206.7 0.0 copy-done.8
  206.7 0.9 fusion.46
  207.6 0.1 all-gather.6.cloned.1.call-update
  207.7 0.0 copy-start.5
  207.7 0.0 copy-start.6
  207.7 22.5 %all-gather.8.cloned.1.call-done = bf16[2048,2112]{0,1:T(8,128)(2,1)} async-done(((bf16[128,2112]{0,1:T(8,128)(2,1)}), bf16[2048,2112]{0,1:T(8,128)(2,1)}) %all-gather.8.cloned.1.call-update) | async-done | bytes 8650768 | tf_op jit(solution)/shard_map/all_gather | solution.py:15
  230.2 42.3 %all-gather.6.cloned.1.call-done = bf16[768,2048]{1,0:T(8,128)(2,1)} async-done(((bf16[96,2048]{1,0:T(8,128)(2,1)}), bf16[768,2048]{1,0:T(8,128)(2,1)}) %all-gather.6.cloned.1.call-update) | async-done | bytes 3145744 | tf_op jit(solution)/shard_map/all_gather | solution.py:132
  272.5 8.4 %fusion.9 = bf16[768,1408]{1,0:T(8,128)(2,1)S(1)} fusion(bf16[768,2048]{1,0:T(8,128)(2,1)} %all-gather.6.cloned.1.call-done, bf16[2048,2112]{0,1:T(8,128)(2,1)} %all-gather.8.cloned.1.call-done), kind=kOutput, calls=%fused_computation.17 | convolution fusion | flops 4430266368 | bytes 11075584 | tf_op jit(solution)/shard_map/dot_general | solution.py:131
  280.9 3.2 collective-permute-start
  284.1 1.3 collective-permute-start.1
  285.4 0.0 copy-done.5
  285.4 0.0 copy-done.6
  285.4 0.1 maximum_reduce_fusion.1
  285.5 0.0 collective-permute-done
  285.6 2.9 collective-permute-done.1
  288.5 0.4 maximum_convert_fusion
  288.9 1.3 fusion.7
  290.2 5.1 %convolution_convert_fusion = bf16[768,2048]{1,0:T(8,128)(2,1)S(1)} fusion(bf16[2048,2112]{0,1:T(8,128)(2,1)} %all-gather.8.cloned.1.call-done, f32[768,1408]{1,0:T(8,128)S(1)} %fusion.7), kind=kOutput, calls=%fused_computation.15 | convolution fusion | flops 2221572096 | bytes 10747904 | tf_op jit(solution)/shard_map/dot_general | solution.py:143
  295.3 0.0 copy-start.1
  295.3 42.0 %all_to_all.11 = bf16[8,96,2048]{2,1,0:T(8,128)(2,1)S(1)} all-to-all(bf16[8,96,2048]{2,1,0:T(8,128)(2,1)S(1)} %bitcast.15), channel_id=1, replica_groups=mesh['grp'=2,'sp'=16,'tp'=8] {'tp'}, dimensions={0} | all-to-all | bytes 6291456 | tf_op jit(solution)/shard_map/all_to_all | solution.py:29
  337.3 0.6 convert_reduce_fusion
  337.9 0.8 fusion.47
  338.7 0.0 copy-done.1
  (8 shorter events, 0.1 us)
Async XLA Ops:
  6.5 134.7 %copy-start = (bf16[128,2048]{1,0:T(8,128)(2,1)S(1)}, bf16[128,2048]{1,0:T(8,128)(2,1)}, u32[]{:S(2)}) copy-start(bf16[128,2048]{1,0:T(8,128)(2,1)} %param.20) | copy-start | bytes 1572868
  6.6 4.0 %copy-start.3 = (bf16[768,256]{1,0:T(8,128)(2,1)S(1)}, bf16[768,256]{1,0:T(8,128)(2,1)}, u32[]{:S(2)}) copy-start(bf16[768,256]{1,0:T(8,128)(2,1)} %param.15) | copy-start | bytes 1179652
  6.6 4.0 %copy-start.10 = (f32[128]{0:T(128)S(1)}, f32[128]{0:T(128)}, u32[]{:S(2)}) copy-start(f32[128]{0:T(128)} %param.18) | copy-start | bytes 1540
  6.6 103.0 %all-gather.4.cloned.1.call-start = ((), (), s32[]{:S(2)}) async-start(), calls=%async_computation.2 | async-start | bytes 6684672 | tf_op jit(solution)/shard_map/all_gather | solution.py:15
  8.9 6.6 %copy-start.2 = (bf16[768,128]{1,0:T(8,128)(2,1)S(1)}, bf16[768,128]{1,0:T(8,128)(2,1)}, u32[]{:S(2)}) copy-start(bf16[768,128]{1,0:T(8,128)(2,1)} %param.14) | copy-start | bytes 589828
  8.9 6.8 %copy-start.9 = (f32[128]{0:T(128)S(1)}, f32[128]{0:T(128)}, u32[]{:S(2)}) copy-start(f32[128]{0:T(128)} %param.17) | copy-start | bytes 1540
  13.4 216.8 %all-gather.8.cloned.1.call-start = ((), (), s32[]{:S(2)}) async-start(), calls=%async_computation.4 | async-start | bytes 9191424 | tf_op jit(solution)/shard_map/all_gather | solution.py:15
  15.5 257.0 %all-gather.6.cloned.1.call-start = ((), (), s32[]{:S(2)}) async-start(), calls=%async_computation.3 | async-start | bytes 3538944 | tf_op jit(solution)/shard_map/all_gather | solution.py:132
  159.9 46.4 %copy-start.4 = (bf16[96,2048]{1,0:T(8,128)(2,1)S(1)}, bf16[96,2048]{1,0:T(8,128)(2,1)}, u32[]{:S(2)}) copy-start(bf16[96,2048]{1,0:T(8,128)(2,1)} %param.19) | copy-start | bytes 1179652
  159.9 46.4 %copy-start.7 = (f32[2048]{0:T(1024)S(1)}, f32[2048]{0:T(1024)}, u32[]{:S(2)}) copy-start(f32[2048]{0:T(1024)} %param.21) | copy-start | bytes 24580
  205.6 1.1 copy-start.8
  207.7 77.8 %copy-start.5 = (f32[3,704]{1,0:T(4,128)S(1)}, f32[3,704]{1,0:T(4,128)}, u32[]{:S(2)}) copy-start(f32[3,704]{1,0:T(4,128)} %param.26) | copy-start | bytes 25348
  207.7 77.8 %copy-start.6 = (f32[3,704]{1,0:T(4,128)S(1)}, f32[3,704]{1,0:T(4,128)}, u32[]{:S(2)}) copy-start(f32[3,704]{1,0:T(4,128)} %param.25) | copy-start | bytes 25348
  280.9 4.6 %collective-permute-start = (bf16[1,1408]{1,0:T(2,128)(2,1)S(1)}, bf16[1,1408]{1,0:T(2,128)(2,1)S(1)}, u32[]{:S(2)}, u32[]{:S(2)}) collective-permute-start(bf16[1,1408]{1,0:T(2,128)(2,1)S(1)} %get-tuple-element.10), channel_id=1, source_target_pairs={{0,8},{8,16},{16,24},{24,32},{32,40},{40,48},{48,56},{56,64},{64,7... | collective-permute-start | bytes 8456 | tf_op jit(solution)/shard_map/ppermute | solution.py:38
  284.1 4.4 %collective-permute-start.1 = (bf16[1,1408]{1,0:T(2,128)(2,1)S(1)}, bf16[1,1408]{1,0:T(2,128)(2,1)S(1)}, u32[]{:S(2)}, u32[]{:S(2)}) collective-permute-start(bf16[1,1408]{1,0:T(2,128)(2,1)S(1)} %get-tuple-element.11), channel_id=1, source_target_pairs={{8,0},{16,8},{24,16},{32,24},{40,32},{48,40},{56,48},{64,56},{72,6... | collective-permute-start | bytes 8456 | tf_op jit(solution)/shard_map/ppermute | solution.py:41
  295.3 43.4 %copy-start.1 = (bf16[128,2048]{1,0:T(8,128)(2,1)S(1)}, bf16[128,2048]{1,0:T(8,128)(2,1)}, u32[]{:S(2)}) copy-start(bf16[128,2048]{1,0:T(8,128)(2,1)} %param.20) | copy-start | bytes 1572868
Sparse Core Ops, SparseCore 0:
  13.5 95.9 all-gather.3
  111.3 118.8 all-gather.7
  232.0 40.3 all-gather.5
where the time goes:
time: 346 us; the launch traced here: 345 us
  waiting for transfers between devices  161 us (47%)
  blocking collectives  87.7 us (25%)
  matrix products  48.5 us (14%)
  other arithmetic  28.9 us (8%)
  between operations  13.4 us (4%)
  starting transfers between devices  4.63 us (1%)
    all_gather x2, waiting for transfers between devices, sent_together(): lax.all_gather(both, axis, axis=dim, tiled=True)  116 us
    all_to_all x2, blocking collectives, summed_on_arrival(): lax.all_to_all(tiles, axis, split_axis=0, concat_axis=0, tiled=True)  87.7 us
    all_gather x1, waiting for transfers between devices, body(): lax.all_gather(normed, 'tp', axis=0, tiled=True)  42.3 us
    dot_general x1, matrix products, body(): jnp.dot(block_rows, out_weight, preferred_element_type=jnp.float32)  18.7 us
    dot_general x1, matrix products, body(): lax.dot_general(query_rows, key_piece, (((1,), (1,)), ((), ())), preferre...  16.3 us
    reduce_sum x1, other arithmetic, body(): denom = jnp.sum(weights, axis=1, keepdims=True)  15.4 us
    dot_general x1, matrix products, body(): jnp.dot(lax.all_gather(normed, 'tp', axis=0, tiled=True), paired, preferr...  8.42 us
  transfers between devices with their start and end apart: 5, of which 4 were waited for; matrix products, arithmetic and copies ran while one was open for 16% of the time, Pallas kernels for 0%

commit v1 on v0

--- a/solution.py
+++ b/solution.py
@@ -1,3 +1,4 @@
+import functools
 import jax
 import jax.numpy as jnp
 from jax import lax
@@ -8,6 +9,21 @@
 GRID_W = 64
 EPSILON = 1e-06
 THETA = 10000.0
+
+
+def play_hubs(own_rows, dev_axis):
+    n_slots = lax.axis_size(dev_axis)
+    rr = 0
+    entries = []
+    while rr < own_rows.ndim:
+        entries.append(n_slots if rr == 0 else 1)
+        rr = rr + 1
+    a_now = jnp.tile(own_rows, entries)
+    f_next = lax.all_to_all(a_now, dev_axis, split_axis=0, tiled=True, concat_axis=0)
+    return f_next
+
+
+_write_units = functools.partial(play_hubs, dev_axis="tp")
 
 
 def sent_together(arrays, axis, dim, along):
@@ -128,9 +144,9 @@
     stream = (residual.astype(jnp.float32) + rms_rows(mix, mix_gain)).astype(jnp.bfloat16)
     normed = rms_rows(stream, ffn_gain).astype(jnp.bfloat16)
     paired = jnp.concatenate([gate_rows, value_rows], axis=1)
-    upward = jnp.dot(
-        lax.all_gather(normed, "tp", axis=0, tiled=True), paired, preferred_element_type=jnp.float32
-    ).astype(jnp.bfloat16)
+    upward = jnp.dot(_write_units(normed), paired, preferred_element_type=jnp.float32).astype(
+        jnp.bfloat16
+    )
     padded = with_halo(upward, (("sp", 0),), 1).astype(jnp.float32)
     taps = jnp.concatenate([conv_gate, conv_value], axis=1)
     mixed = taps[0] * padded[:-2] + taps[1] * padded[1:-1] + taps[2] * padded[2:]

time: 346 us -> 325 us (0.939)
  waiting for transfers between devices: 161 us -> 134 us
  starting transfers between devices: 4.63 us -> 8.99 us
    all_gather x1 -> x0, waiting for transfers between devices: 42.3 us -> none  [body(): lax.all_gather(normed, 'tp', axis=0, tiled=True)]
    all_to_all x0 -> x1, waiting for transfers between devices: none -> 21.7 us  [play_hubs(): lax.all_to_all(a_now, dev_axis, split_axis=0, tiled=True, concat_axis=0)]
    all_gather x2, waiting for transfers between devices: 116 us -> 109 us  [sent_together(): lax.all_gather(both, axis, axis=dim, tiled=True)]
    all_to_all x0 -> x1, starting transfers between devices: none -> 5.31 us  [play_hubs(): lax.all_to_all(a_now, dev_axis, split_axis=0, tiled=True, concat_axis=0)]
  transfers between devices with their start and end apart: 5 -> 5, of which waited for: 4 -> 4; matrix products, arithmetic and copies ran while one was open for 16% -> 17% of each run, Pallas kernels for 0% -> 0%
where the time goes in v1:
time: 325 us
  waiting for transfers between devices  134 us (41%)
  blocking collectives  88.2 us (27%)
  matrix products  48.5 us (15%)
  other arithmetic  28.1 us (9%)
  between operations  13.7 us (4%)
  starting transfers between devices  8.99 us (3%)
    all_gather x2, waiting for transfers between devices, sent_together(): lax.all_gather(both, axis, axis=dim, tiled=True)  109 us
    all_to_all x2, blocking collectives, summed_on_arrival(): lax.all_to_all(tiles, axis, split_axis=0, concat_axis=0, tiled=True)  88.2 us
    all_to_all x1, waiting for transfers between devices, play_hubs(): lax.all_to_all(a_now, dev_axis, split_axis=0, tiled=True, concat_axis=0)  21.7 us
    dot_general x1, matrix products, body(): jnp.dot(block_rows, out_weight, preferred_element_type=jnp.float32)  18.7 us
    dot_general x1, matrix products, body(): lax.dot_general(query_rows, key_piece, (((1,), (1,)), ((), ())), preferre...  16.3 us
    reduce_sum x1, other arithmetic, body(): denom = jnp.sum(weights, axis=1, keepdims=True)  15.4 us
    dot_general x1, matrix products, body(): jnp.dot(_write_units(normed), paired, preferred_element_type=jnp.float32)  8.44 us
  transfers between devices with their start and end apart: 5, of which 4 were waited for; matrix products, arithmetic and copies ran while one was open for 17% of the time, Pallas kernels for 0%

profile of v1, /device:TPU:33, one launch (start us, length us, event | category | flops | bytes accessed | tf_op | source)
XLA Modules:
  0.0 324.6 jit_solution(421767401948182054)
XLA Ops:
  6.5 0.0 copy-start
  6.6 0.0 copy-start.3
  6.6 0.0 copy-start.10
  6.6 0.0 all-gather.3.cloned.1.call-start
  6.6 1.2 fusion.55
  7.8 1.1 fusion.56
  8.9 0.0 copy-start.2
  8.9 0.0 copy-start.9
  8.9 0.4 slice_negate_fusion.1
  9.3 0.9 constant_dynamic-slice_fusion
  10.3 0.3 broadcast_multiply_fusion.1
  10.6 0.0 copy-done.3
  10.6 0.0 copy-done.10
  10.6 2.0 fusion.60
  12.6 0.8 pad_maximum_fusion.2
  13.4 0.1 all-gather.3.cloned.1.call-update
  13.4 0.1 all-gather.5.cloned.1.call-start
  13.5 1.9 pad_maximum_fusion
  15.4 0.1 all-gather.5.cloned.1.call-update
  15.5 0.0 copy-done.2
  15.5 0.2 fusion.48
  15.7 0.0 copy-done.9
  15.7 0.2 fusion.50
  15.9 0.4 fusion.58
  16.3 93.3 %all-gather.3.cloned.1.call-done = bf16[12288,256]{1,0:T(8,128)(2,1)} async-done(((bf16[768,256]{1,0:T(8,128)(2,1)}), bf16[12288,256]{1,0:T(8,128)(2,1)}) %all-gather.3.cloned.1.call-update) | async-done | bytes 6291472 | tf_op jit(solution)/shard_map/all_gather | solution.py:31
  109.5 16.3 %fusion.87 = (f32[768]{0:T(1024)S(1)}, f32[768,12288]{1,0:T(8,128)}) fusion(bf16[12288,256]{1,0:T(8,128)(2,1)} %all-gather.3.cloned.1.call-done, bf16[768,128]{1,0:T(8,128)(2,1)S(1)} %copy-done.2, f32[768,32]{1,0:T(8,128)S(1)} %get-tuple-element.13, f32[768,32]{1,0:T(8,128)S(1)} %get-tuple-element.14, f32[768,32]{1,0:T(8,128)S(1)} %get-tuple-element.15, ...), kind=kOutput, calls=%fused_computation.117 | convolution fusion | flops 2426731776 | bytes 41687552 | tf_op jit(solution)/shard_map/dot_general | solution.py:128
  125.9 15.4 %fusion = f32[768]{0:T(1024)S(1)} fusion(f32[768,12288]{1,0:T(8,128)} %get-tuple-element.23, f32[768]{0:T(1024)S(1)} %broadcast_maximum_fusion), kind=kLoop, calls=%fused_computation.1 | loop fusion | flops 18873600 | bytes 37754880 | tf_op jit(solution)/shard_map/reduce_sum | solution.py:133
  141.2 0.0 copy-done
  141.2 18.7 %convolution_convert_fusion.1 = bf16[768,2048]{1,0:T(8,128)(2,1)} fusion(bf16[128,2048]{1,0:T(8,128)(2,1)S(1)} %copy-done, bf16[12288,256]{1,0:T(8,128)(2,1)} %all-gather.3.cloned.1.call-done, f32[768,12288]{1,0:T(8,128)} %get-tuple-element.23, f32[768]{0:T(1024)S(1)} %broadcast_maximum_fusion, f32[768]{0:T(1024)S(1)} %fusion), kind=kOutput, calls=%fused_computation.16 | convolution fusion | flops 2839216128 | bytes 44570624 | tf_op jit(solution)/shard_map/dot_general | solution.py:140
  159.9 0.0 copy-start.4
  159.9 0.0 copy-start.7
  159.9 45.7 %all_to_all.19 = bf16[8,96,2048]{2,1,0:T(8,128)(2,1)S(1)} all-to-all(bf16[8,96,2048]{2,1,0:T(8,128)(2,1)} %bitcast.15), channel_id=1, replica_groups=mesh['grp'=2,'sp'=16,'tp'=8] {'tp'}, dimensions={0} | all-to-all | bytes 6291456 | tf_op jit(solution)/shard_map/all_to_all | solution.py:45
  205.6 0.0 copy-start.8
  205.6 0.6 convert_reduce_fusion.1
  206.2 0.1 multiply_reduce_fusion
  206.3 0.0 copy-done.4
  206.3 0.0 copy-done.7
  206.3 0.3 fusion.44
  206.7 0.0 copy-done.8
  206.7 0.2 fusion.46
  206.9 2.1 tile.2
  209.0 5.3 %all-to-all-start.1 = ((bf16[8,96,2048]{2,1,0:T(8,128)(2,1)}), bf16[8,96,2048]{2,1,0:T(8,128)(2,1)}, u32[]{:S(2)}, u32[]{:S(2)}) async-start(bf16[8,96,2048]{2,1,0:T(8,128)(2,1)} %tile.2), calls=%async_computation.1 | async-start | bytes 6291456 | tf_op jit(solution)/shard_map/all_to_all | solution.py:22
  214.3 15.9 %all-gather.5.cloned.1.call-done = bf16[2048,2112]{0,1:T(8,128)(2,1)} async-done(((bf16[128,2112]{0,1:T(8,128)(2,1)}), bf16[2048,2112]{0,1:T(8,128)(2,1)}) %all-gather.5.cloned.1.call-update) | async-done | bytes 8650768 | tf_op jit(solution)/shard_map/all_gather | solution.py:31
  230.2 21.7 %all-to-all-done.1 = bf16[8,96,2048]{2,1,0:T(8,128)(2,1)} async-done(((bf16[8,96,2048]{2,1,0:T(8,128)(2,1)}), bf16[8,96,2048]{2,1,0:T(8,128)(2,1)}, u32[]{:S(2)}, u32[]{:S(2)}) %all-to-all-start.1) | async-done | bytes 3145760 | tf_op jit(solution)/shard_map/all_to_all | solution.py:22
  251.9 0.0 copy-start.5
  251.9 0.0 copy-start.6
  251.9 8.4 %fusion.9 = bf16[768,1408]{1,0:T(8,128)(2,1)S(1)} fusion(bf16[768,2048]{1,0:T(8,128)(2,1)} %bitcast.6, bf16[2048,2112]{0,1:T(8,128)(2,1)} %all-gather.5.cloned.1.call-done), kind=kOutput, calls=%fused_computation.17 | convolution fusion | flops 4430266368 | bytes 11075584 | tf_op jit(solution)/shard_map/dot_general | solution.py:147
  260.4 2.3 collective-permute-start
  262.7 1.3 collective-permute-start.1
  264.0 0.0 copy-done.5
  264.0 0.0 copy-done.6
  264.0 0.1 maximum_reduce_fusion.1
  264.1 0.0 collective-permute-done
  264.1 2.9 collective-permute-done.1
  267.1 0.4 maximum_convert_fusion
  267.5 1.3 fusion.7
  268.8 5.1 %convolution_convert_fusion = bf16[768,2048]{1,0:T(8,128)(2,1)S(1)} fusion(bf16[2048,2112]{0,1:T(8,128)(2,1)} %all-gather.5.cloned.1.call-done, f32[768,1408]{1,0:T(8,128)S(1)} %fusion.7), kind=kOutput, calls=%fused_computation.15 | convolution fusion | flops 2221572096 | bytes 10747904 | tf_op jit(solution)/shard_map/dot_general | solution.py:159
  273.9 0.0 copy-start.1
  273.9 42.5 %all_to_all.20 = bf16[8,96,2048]{2,1,0:T(8,128)(2,1)S(1)} all-to-all(bf16[8,96,2048]{2,1,0:T(8,128)(2,1)S(1)} %bitcast.16), channel_id=1, replica_groups=mesh['grp'=2,'sp'=16,'tp'=8] {'tp'}, dimensions={0} | all-to-all | bytes 6291456 | tf_op jit(solution)/shard_map/all_to_all | solution.py:45
  316.4 0.6 convert_reduce_fusion
  316.9 0.8 fusion.47
  317.8 0.0 copy-done.1
  (8 shorter events, 0.1 us)
Async XLA Ops:
  6.5 134.7 %copy-start = (bf16[128,2048]{1,0:T(8,128)(2,1)S(1)}, bf16[128,2048]{1,0:T(8,128)(2,1)}, u32[]{:S(2)}) copy-start(bf16[128,2048]{1,0:T(8,128)(2,1)} %param.20) | copy-start | bytes 1572868
  6.6 4.0 %copy-start.3 = (bf16[768,256]{1,0:T(8,128)(2,1)S(1)}, bf16[768,256]{1,0:T(8,128)(2,1)}, u32[]{:S(2)}) copy-start(bf16[768,256]{1,0:T(8,128)(2,1)} %param.15) | copy-start | bytes 1179652
  6.6 4.0 %copy-start.10 = (f32[128]{0:T(128)S(1)}, f32[128]{0:T(128)}, u32[]{:S(2)}) copy-start(f32[128]{0:T(128)} %param.18) | copy-start | bytes 1540
  6.6 103.0 %all-gather.3.cloned.1.call-start = ((), (), s32[]{:S(2)}) async-start(), calls=%async_computation.3 | async-start | bytes 6684672 | tf_op jit(solution)/shard_map/all_gather | solution.py:31
  8.9 6.6 %copy-start.2 = (bf16[768,128]{1,0:T(8,128)(2,1)S(1)}, bf16[768,128]{1,0:T(8,128)(2,1)}, u32[]{:S(2)}) copy-start(bf16[768,128]{1,0:T(8,128)(2,1)} %param.14) | copy-start | bytes 589828
  8.9 6.8 %copy-start.9 = (f32[128]{0:T(128)S(1)}, f32[128]{0:T(128)}, u32[]{:S(2)}) copy-start(f32[128]{0:T(128)} %param.17) | copy-start | bytes 1540
  13.4 216.8 %all-gather.5.cloned.1.call-start = ((), (), s32[]{:S(2)}) async-start(), calls=%async_computation.4 | async-start | bytes 9191424 | tf_op jit(solution)/shard_map/all_gather | solution.py:31
  159.9 46.4 %copy-start.4 = (bf16[96,2048]{1,0:T(8,128)(2,1)S(1)}, bf16[96,2048]{1,0:T(8,128)(2,1)}, u32[]{:S(2)}) copy-start(bf16[96,2048]{1,0:T(8,128)(2,1)} %param.19) | copy-start | bytes 1179652
  159.9 46.4 %copy-start.7 = (f32[2048]{0:T(1024)S(1)}, f32[2048]{0:T(1024)}, u32[]{:S(2)}) copy-start(f32[2048]{0:T(1024)} %param.21) | copy-start | bytes 24580
  205.6 1.1 copy-start.8
  209.0 42.9 %all-to-all-start.1 = ((bf16[8,96,2048]{2,1,0:T(8,128)(2,1)}), bf16[8,96,2048]{2,1,0:T(8,128)(2,1)}, u32[]{:S(2)}, u32[]{:S(2)}) async-start(bf16[8,96,2048]{2,1,0:T(8,128)(2,1)} %tile.2), calls=%async_computation.1 | async-start | bytes 6291456 | tf_op jit(solution)/shard_map/all_to_all | solution.py:22
  251.9 12.1 %copy-start.5 = (f32[3,704]{1,0:T(4,128)S(1)}, f32[3,704]{1,0:T(4,128)}, u32[]{:S(2)}) copy-start(f32[3,704]{1,0:T(4,128)} %param.26) | copy-start | bytes 25348
  251.9 12.1 %copy-start.6 = (f32[3,704]{1,0:T(4,128)S(1)}, f32[3,704]{1,0:T(4,128)}, u32[]{:S(2)}) copy-start(f32[3,704]{1,0:T(4,128)} %param.25) | copy-start | bytes 25348
  260.4 3.8 %collective-permute-start = (bf16[1,1408]{1,0:T(2,128)(2,1)S(1)}, bf16[1,1408]{1,0:T(2,128)(2,1)S(1)}, u32[]{:S(2)}, u32[]{:S(2)}) collective-permute-start(bf16[1,1408]{1,0:T(2,128)(2,1)S(1)} %get-tuple-element.10), channel_id=1, source_target_pairs={{0,8},{8,16},{16,24},{24,32},{32,40},{40,48},{48,56},{56,64},{64,7... | collective-permute-start | bytes 8456 | tf_op jit(solution)/shard_map/ppermute | solution.py:54
  262.7 4.4 %collective-permute-start.1 = (bf16[1,1408]{1,0:T(2,128)(2,1)S(1)}, bf16[1,1408]{1,0:T(2,128)(2,1)S(1)}, u32[]{:S(2)}, u32[]{:S(2)}) collective-permute-start(bf16[1,1408]{1,0:T(2,128)(2,1)S(1)} %get-tuple-element.11), channel_id=1, source_target_pairs={{8,0},{16,8},{24,16},{32,24},{40,32},{48,40},{56,48},{64,56},{72,6... | collective-permute-start | bytes 8456 | tf_op jit(solution)/shard_map/ppermute | solution.py:57
  273.9 43.9 %copy-start.1 = (bf16[128,2048]{1,0:T(8,128)(2,1)S(1)}, bf16[128,2048]{1,0:T(8,128)(2,1)}, u32[]{:S(2)}) copy-start(bf16[128,2048]{1,0:T(8,128)(2,1)} %param.20) | copy-start | bytes 1572868
Sparse Core Ops, SparseCore 0:
  13.5 95.9 all-gather.2
  111.3 118.8 all-gather.4
